TPU v7x, 32 devices: a whole 2x2x4 slice. The times are simulated.
32 devices in a mesh: grp: 2 (over y), sp: 4 (over z), tp: 4 (over x, core).
Axes of the slice: x: 2, y: 2, z: 4, core: 2. Of those that a mesh axis runs over, the one named last changes fastest.
Arguments:
- queries: bfloat16 [6144, 1024], P(('grp', 'sp'), 'tp'), parts along dimension 0, may hold values from -8 to 8
- keys: bfloat16 [6144, 256], P(('grp', 'sp')), parts along dimension 0, may hold values from -8 to 8
- values: bfloat16 [6144, 256], P(('grp', 'sp')), parts along dimension 0, may hold values from -6 to 6
- query_gain: float32 [128], replicated, may hold values from 0.2 to 6
- key_gain: float32 [128], replicated, may hold values from 0.2 to 6
- residual: bfloat16 [6144, 2048], P(('grp', 'sp', 'tp')), parts along dimension 0, may hold values from -6 to 6
- out_weight: bfloat16 [1024, 2048], P('tp'), may hold values from -0.1875 to 0.1875
- mix_gain: float32 [2048], replicated, may hold values from 0.1 to 1.9
- ffn_gain: float32 [2048], replicated, may hold values from 0.1 to 1.9
- gate_in: bfloat16 [2048, 5632], P('sp', 'tp'), may hold values from -0.125 to 0.125
- value_in: bfloat16 [2048, 5632], P('sp', 'tp'), may hold values from -0.125 to 0.125
- conv_gate: float32 [3, 5632], P(None, 'tp'), may hold values from -3 to 3
- conv_value: float32 [3, 5632], P(None, 'tp'), may hold values from -3 to 3
- down_t: bfloat16 [2048, 5632], P('sp', 'tp'), may hold values from -0.078125 to 0.078125
Outputs:
- layer_out: bfloat16 [6144, 2048], P(('grp', 'sp', 'tp')), parts along dimension 0
There are 2 independent parts, one for each index of `grp`. A program takes and returns all parts, laid end to end along the dimension named above; an argument that names none is the same for every part. Nothing has to cross between parts.
All inputs are finite; a program needn't handle non-finite values.
Results may differ from a plain program's by a relative error of at most 0.02.
The roundings to bfloat16 on the way count: a program that leaves them out, or rounds other values in their place, can miss the bound.
Values may be sent and summed in bfloat16 or wider, within the bound.
A program may use at most 128 MiB of HBM per device.

v0:
```python
import jax
import jax.numpy as jnp
from jax import lax
from jax.sharding import PartitionSpec as P

HEADS = 8
KVH = 2
GRID_W = 64
EPSILON = 1e-06
THETA = 10000.0


def with_halo(block, sides, width):
    for axis, dim in sides:
        count = lax.axis_size(axis)
        forward = [(i, i + 1) for i in range(count - 1)]
        backward = [(target, source) for source, target in forward]
        low = lax.ppermute(
            lax.slice_in_dim(block, block.shape[dim] - width, None, axis=dim), axis, forward
        )
        high = lax.ppermute(lax.slice_in_dim(block, 0, width, axis=dim), axis, backward)
        block = jnp.concatenate([low, block, high], axis=dim)
    return block


def rotary_tables(positions, seq_total, head_dim):
    quarter = head_dim // 4
    inverse = THETA ** (-(2.0 * jnp.arange(quarter, dtype=jnp.float32)) / (head_dim // 2))
    grid_row = (positions // GRID_W - seq_total // GRID_W // 2).astype(jnp.float32)
    grid_col = (positions % GRID_W - GRID_W // 2).astype(jnp.float32)
    row_angle = grid_row[:, None] * inverse[None, :]
    col_angle = grid_col[:, None] * inverse[None, :]
    angle = jnp.concatenate([row_angle, row_angle, col_angle, col_angle], axis=-1)
    return (jnp.cos(angle), jnp.sin(angle))


def rotate_quarters(vector):
    first, second, third, fourth = jnp.split(vector, 4, axis=-1)
    return jnp.concatenate([-second, first, -fourth, third], axis=-1)


def prepare_heads(raw, gain, cos_table, sin_table, factor):
    floats = raw.astype(jnp.float32)
    normed = floats * lax.rsqrt(jnp.mean(floats * floats, axis=-1, keepdims=True) + EPSILON) * gain
    turned = normed * cos_table + rotate_quarters(normed) * sin_table
    return (turned * factor).astype(jnp.bfloat16)


def rms_rows(stream, gain):
    floats = stream.astype(jnp.float32)
    return floats * lax.rsqrt(jnp.mean(floats * floats, axis=-1, keepdims=True) + EPSILON) * gain


def body(
    queries,
    keys,
    values,
    query_gain,
    key_gain,
    residual,
    out_weight,
    mix_gain,
    ffn_gain,
    gate_in,
    value_in,
    conv_gate,
    conv_value,
    down_t,
):
    gate_rows, value_rows, down_rows = (
        lax.all_gather(gate_in, "sp", axis=0, tiled=True),
        lax.all_gather(value_in, "sp", axis=0, tiled=True),
        lax.all_gather(down_t, "sp", axis=0, tiled=True),
    )
    whole_out = lax.all_gather(out_weight, "tp", axis=0, tiled=True)
    tok_rows = queries.shape[0]
    head_dim = query_gain.shape[0]
    local_heads = queries.shape[1] // head_dim
    seq_total = tok_rows * lax.axis_size("sp")
    kv_head = lax.axis_index("tp") * local_heads // (HEADS // KVH)
    positions = lax.axis_index("sp") * tok_rows + jnp.arange(tok_rows, dtype=jnp.int32)
    cos_table, sin_table = rotary_tables(positions, seq_total, head_dim)
    key_own = lax.dynamic_slice_in_dim(keys, kv_head * head_dim, head_dim, 1)
    value_own = lax.dynamic_slice_in_dim(values, kv_head * head_dim, head_dim, 1)
    key_rot = prepare_heads(key_own, key_gain, cos_table, sin_table, 1.0)
    query_rot = prepare_heads(
        queries.reshape(tok_rows, local_heads, head_dim),
        query_gain,
        cos_table[:, None, :],
        sin_table[:, None, :],
        head_dim ** (-0.5),
    )
    query_rows = jnp.transpose(query_rot, (1, 0, 2)).reshape(local_heads * tok_rows, head_dim)
    query_count = local_heads * tok_rows
    running = jnp.full((query_count, 1), -1e30, jnp.float32)
    key_piece = lax.all_gather(key_rot, "sp", axis=0, tiled=True)
    value_piece = lax.all_gather(value_own, "sp", axis=0, tiled=True)
    scores = lax.dot_general(
        query_rows, key_piece, (((1,), (1,)), ((), ())), preferred_element_type=jnp.float32
    )
    newest = jnp.maximum(running, jnp.max(scores, axis=1, keepdims=True))
    weights = jnp.exp(scores - newest)
    denom = jnp.sum(weights, axis=1, keepdims=True)
    summed = jnp.dot(weights.astype(jnp.bfloat16), value_piece, preferred_element_type=jnp.float32)
    running, denom, summed = (newest, denom, summed)
    attended = (summed / denom).astype(jnp.bfloat16).reshape(local_heads, tok_rows, head_dim)
    attended = jnp.transpose(attended, (1, 0, 2)).reshape(tok_rows, local_heads * head_dim)
    own_rows = residual.shape[0]
    token_heads = lax.all_to_all(attended, "tp", split_axis=0, concat_axis=1, tiled=True)
    group_count = lax.axis_size("tp")
    group_cols = attended.shape[1]
    grouped_rows = token_heads.reshape(own_rows, group_count, group_cols)
    grouped_weight = whole_out.reshape(group_count, group_cols, whole_out.shape[1])
    partials = jnp.einsum(
        "rgc,gcd->grd", grouped_rows, grouped_weight, preferred_element_type=jnp.float32
    ).astype(jnp.bfloat16)
    mix = jnp.sum(partials.astype(jnp.float32), axis=0)
    stream = (residual.astype(jnp.float32) + rms_rows(mix, mix_gain)).astype(jnp.bfloat16)
    normed = rms_rows(stream, ffn_gain).astype(jnp.bfloat16)
    paired = jnp.concatenate([gate_rows, value_rows], axis=1)
    upward = jnp.dot(
        lax.all_gather(normed, "tp", axis=0, tiled=True), paired, preferred_element_type=jnp.float32
    ).astype(jnp.bfloat16)
    padded = with_halo(upward, (("sp", 0),), 1).astype(jnp.float32)
    taps = jnp.concatenate([conv_gate, conv_value], axis=1)
    mixed = taps[0] * padded[:-2] + taps[1] * padded[1:-1] + taps[2] * padded[2:]
    unit_cols = conv_gate.shape[1]
    hidden = (jax.nn.gelu(mixed[:, :unit_cols], approximate=True) * mixed[:, unit_cols:]).astype(
        jnp.bfloat16
    )
    ffn_out = lax.psum_scatter(
        lax.dot_general(
            hidden, down_rows, (((1,), (1,)), ((), ())), preferred_element_type=jnp.float32
        ).astype(jnp.bfloat16),
        "tp",
        scatter_dimension=0,
        tiled=True,
    ).astype(jnp.float32)
    return (stream.astype(jnp.float32) + ffn_out).astype(jnp.bfloat16)


def solution(mesh):
    return jax.shard_map(
        body,
        mesh=mesh,
        in_specs=(
            P(("grp", "sp"), "tp"),
            P(("grp", "sp"), None),
            P(("grp", "sp"), None),
            P(),
            P(),
            P(("grp", "sp", "tp"), None),
            P("tp", None),
            P(),
            P(),
            P("sp", "tp"),
            P("sp", "tp"),
            P(None, "tp"),
            P(None, "tp"),
            P("sp", "tp"),
        ),
        out_specs=P(("grp", "sp", "tp"), None),
        check_vma=False,
    )
```

profile of v0, /device:TPU:0, one launch (start us, length us, event | category | flops | bytes accessed | tf_op | source)
XLA Modules:
  0.0 454.8 jit_solution(9116688480287603135)
XLA Ops:
  6.5 0.7 all-gather.6.cloned.1.call-update
  7.3 0.7 all-gather.10.cloned.1.call-update
  8.0 0.0 all-gather.12.cloned.1.call-start
  8.1 0.7 all-gather.12.cloned.1.call-update
  8.7 0.0 all-gather.8.cloned.1.call-start
  8.8 1.1 fusion.43
  10.0 1.1 fusion.44
  11.1 0.3 broadcast_multiply_fusion.1
  11.4 0.4 slice_negate_fusion.1
  11.8 2.0 fusion.46
  13.8 0.2 copy.18
  13.9 0.2 copy.19
  14.1 0.2 copy.17
  14.3 0.1 fusion.38
  14.4 0.1 fusion.39
  14.6 0.1 slice_negate_fusion.3
  14.6 0.3 fusion.48
  14.9 0.2 copy.20
  15.2 21.3 %all_gather.21 = bf16[3072,128]{1,0:T(8,128)(2,1)S(1)} all-gather(bf16[768,128]{1,0:T(8,128)(2,1)S(1)} %get-tuple-element.10), channel_id=1, replica_groups=mesh['grp'=2,'sp'=4,'tp'=4] {'sp'}, dimensions={0}, use_global_device_ids=true | all-gather | bytes 983040 | tf_op jit(solution)/shard_map/all_gather | solution.py:96
  36.5 8.0 %fusion.68 = (f32[1536]{0:T(1024)S(1)}, f32[1536,3072]{1,0:T(8,128)}) fusion(bf16[1536,128]{1,0:T(8,128)(2,1)S(1)} %bitcast.24, bf16[3072,128]{1,0:T(8,128)(2,1)S(1)} %all_gather.21), kind=kOutput, calls=%fused_computation.104 | convolution fusion | flops 1212676608 | bytes 20060160 | tf_op jit(solution)/shard_map/dot_general | solution.py:98
  44.5 18.4 %all_gather.22 = bf16[3072,128]{1,0:T(8,128)(2,1)S(1)} all-gather(bf16[768,128]{1,0:T(8,128)(2,1)S(1)} %constant_dynamic-slice_fusion), channel_id=1, replica_groups=mesh['grp'=2,'sp'=4,'tp'=4] {'sp'}, dimensions={0}, use_global_device_ids=true | all-gather | bytes 983040 | tf_op jit(solution)/shard_map/all_gather | solution.py:97
  62.8 9.0 %fusion = f32[1536]{0:T(1024)S(1)} fusion(f32[1536,3072]{1,0:T(8,128)} %get-tuple-element.26, f32[1536]{0:T(1024)S(1)} %broadcast_maximum_fusion), kind=kLoop, calls=%fused_computation.1 | loop fusion | flops 9435648 | bytes 18886656 | tf_op jit(solution)/shard_map/reduce_sum | solution.py:103
  71.9 9.2 %fusion.26 = bf16[1536,128]{1,0:T(8,128)(2,1)S(1)} fusion(bf16[3072,128]{1,0:T(8,128)(2,1)S(1)} %all_gather.22, f32[1536,3072]{1,0:T(8,128)} %get-tuple-element.26, f32[1536]{0:T(1024)S(1)} %broadcast_maximum_fusion, f32[1536]{0:T(1024)S(1)} %fusion), kind=kOutput, calls=%fused_computation.30 | convolution fusion | flops 1217789952 | bytes 20066304 | tf_op jit(solution)/shard_map/dot_general | solution.py:104
  81.1 0.4 copy.21
  81.5 0.3 all_to_all.12
  81.8 9.9 %all_to_all.16 = bf16[4,192,256]{2,1,0:T(8,128)(2,1)S(1)} all-to-all(bf16[4,192,256]{2,1,0:T(8,128)(2,1)S(1)} %all_to_all.12), channel_id=1, replica_groups=mesh['grp'=2,'sp'=4,'tp'=4] {'tp'}, dimensions={0} | all-to-all | bytes 786432 | tf_op jit(solution)/shard_map/all_to_all | solution.py:109
  91.7 3.3 convert_reduce_fusion
  95.1 0.2 multiply_reduce_fusion
  95.3 0.5 fusion.34
  95.8 1.1 fusion.36
  97.0 0.0 all-gather.14.cloned.1.call-start
  97.0 0.5 all-gather.14.cloned.1.call-update
  97.5 0.0 reduce-scatter.2.cloned.1.call-start
  97.6 57.5 %all-gather.10.cloned.1.call-done = bf16[2048,1408]{1,0:T(8,128)(2,1)} async-done(((bf16[512,1408]{1,0:T(8,128)(2,1)}), bf16[2048,1408]{1,0:T(8,128)(2,1)}) %all-gather.10.cloned.1.call-update) | async-done | bytes 5767184 | tf_op jit(solution)/shard_map/all_gather | solution.py:71
  155.1 106.9 %all-gather.12.cloned.1.call-done = bf16[2048,1408]{1,0:T(8,128)(2,1)} async-done(((bf16[512,1408]{1,0:T(8,128)(2,1)}), bf16[2048,1408]{1,0:T(8,128)(2,1)}) %all-gather.12.cloned.1.call-update) | async-done | bytes 5767184 | tf_op jit(solution)/shard_map/all_gather | solution.py:72
  262.0 28.2 %all-gather.8.cloned.1.call-done = bf16[768,2048]{1,0:T(8,128)(2,1)} async-done(((bf16[192,2048]{1,0:T(8,128)(2,1)}), bf16[768,2048]{1,0:T(8,128)(2,1)}) %all-gather.8.cloned.1.call-update) | async-done | bytes 3145744 | tf_op jit(solution)/shard_map/all_gather | solution.py:122
  290.2 13.8 %fusion.11 = bf16[768,2816]{1,0:T(8,128)(2,1)S(1)} fusion(bf16[768,2048]{1,0:T(8,128)(2,1)} %all-gather.8.cloned.1.call-done, bf16[2048,1408]{1,0:T(8,128)(2,1)} %all-gather.12.cloned.1.call-done, bf16[2048,1408]{1,0:T(8,128)(2,1)} %all-gather.10.cloned.1.call-done), kind=kOutput, calls=%fused_computation.16 | convolution fusion | flops 8883601408 | bytes 19005440 | tf_op jit(solution)/shard_map/dot_general | solution.py:121
  304.1 3.4 collective-permute-start
  307.5 1.3 collective-permute-start.1
  308.8 0.1 slice_reduce_fusion.2
  308.9 0.1 collective-permute-done
  309.0 4.5 collective-permute-done.1
  313.5 1.2 maximum_convert_fusion
  314.7 4.7 %fusion.9 = f32[768,2816]{1,0:T(8,128)} fusion(f32[770,2816]{1,0:T(8,128)S(1)} %maximum_convert_fusion, f32[2816]{0:T(1024)S(1)} %get-tuple-element.6, f32[2816]{0:T(1024)S(1)} %get-tuple-element.7, f32[2816]{0:T(1024)S(1)} %get-tuple-element.5), kind=kLoop, calls=%fused_computation.10 | loop fusion | flops 10813440 | bytes 34636800 | tf_op jit(solution)/shard_map/add | solution.py:126
  319.4 79.2 %all-gather.14.cloned.1.call-done = bf16[2048,1408]{1,0:T(8,128)(2,1)} async-done(((bf16[512,1408]{1,0:T(8,128)(2,1)}), bf16[2048,1408]{1,0:T(8,128)(2,1)}) %all-gather.14.cloned.1.call-update) | async-done | bytes 5767184 | tf_op jit(solution)/shard_map/all_gather | solution.py:73
  398.6 10.8 %convolution_convert_fusion.1 = bf16[768,2048]{1,0:T(8,128)(2,1)} fusion(bf16[2048,1408]{1,0:T(8,128)(2,1)} %all-gather.14.cloned.1.call-done, f32[768,2816]{1,0:T(8,128)} %fusion.9), kind=kOutput, calls=%fused_computation.28 | convolution fusion | flops 4441571328 | bytes 17563648 | tf_op jit(solution)/shard_map/dot_general | solution.py:132
  409.4 36.2 %reduce-scatter.2.cloned.1.call-done = bf16[192,2048]{1,0:T(8,128)(2,1)} async-done(((bf16[768,2048]{1,0:T(8,128)(2,1)}), bf16[192,2048]{1,0:T(8,128)(2,1)}) %reduce-scatter.2.cloned.1.call-update) | async-done | bytes 786448 | tf_op jit(solution)/shard_map/reduce_scatter | solution.py:131
  445.6 2.3 fusion.37
  (38 shorter events, 0.3 us)
Async XLA Ops:
  6.5 8.6 %copy-start = (bf16[768,256]{1,0:T(8,128)(2,1)S(1)}, bf16[768,256]{1,0:T(8,128)(2,1)}, u32[]{:S(2)}) copy-start(bf16[768,256]{1,0:T(8,128)(2,1)} %param.16) | copy-start | bytes 1179652
  6.5 5.2 %copy-start.2 = (bf16[768,256]{1,0:T(8,128)(2,1)S(1)}, bf16[768,256]{1,0:T(8,128)(2,1)}, u32[]{:S(2)}) copy-start(bf16[768,256]{1,0:T(8,128)(2,1)} %param.15) | copy-start | bytes 1179652
  6.5 5.2 %copy-start.9 = (f32[128]{0:T(128)S(1)}, f32[128]{0:T(128)}, u32[]{:S(2)}) copy-start(f32[128]{0:T(128)} %param.18) | copy-start | bytes 1540
  6.5 85.2 %all-gather.6.cloned.1.call-start = ((), (), s32[]{:S(2)}) async-start(), calls=%async_computation.2 | async-start | bytes 5242880 | tf_op jit(solution)/shard_map/all_gather | solution.py:75
  7.3 147.8 %all-gather.10.cloned.1.call-start = ((), (), s32[]{:S(2)}) async-start(), calls=%async_computation.4 | async-start | bytes 7208960 | tf_op jit(solution)/shard_map/all_gather | solution.py:71
  8.0 254.0 %all-gather.12.cloned.1.call-start = ((), (), s32[]{:S(2)}) async-start(), calls=%async_computation.5 | async-start | bytes 7208960 | tf_op jit(solution)/shard_map/all_gather | solution.py:72
  8.7 281.5 %all-gather.8.cloned.1.call-start = ((), (), s32[]{:S(2)}) async-start(), calls=%async_computation.3 | async-start | bytes 3932160 | tf_op jit(solution)/shard_map/all_gather | solution.py:122
  11.1 3.0 copy-start.4
  11.4 3.0 copy-start.10
  91.7 3.6 copy-start.3
  91.7 3.6 copy-start.7
  95.0 0.7 copy-start.8
  95.1 2.5 copy-start.5
  95.1 2.5 copy-start.6
  97.0 301.6 %all-gather.14.cloned.1.call-start = ((), (), s32[]{:S(2)}) async-start(), calls=%async_computation.6 | async-start | bytes 7208960 | tf_op jit(solution)/shard_map/all_gather | solution.py:73
  97.5 348.1 %reduce-scatter.2.cloned.1.call-start = ((), (), s32[]{:S(2)}) async-start(), calls=%async_computation.7 | async-start | bytes 3932160 | tf_op jit(solution)/shard_map/reduce_scatter | solution.py:131
  304.1 4.9 %collective-permute-start = (bf16[1,2816]{1,0:T(2,128)(2,1)S(1)}, bf16[1,2816]{1,0:T(2,128)(2,1)S(1)}, u32[]{:S(2)}, u32[]{:S(2)}) collective-permute-start(bf16[1,2816]{1,0:T(2,128)(2,1)S(1)} %get-tuple-element.13), channel_id=1, source_target_pairs={{0,4},{4,8},{8,12},{1,5},{5,9},{9,13},{2,6},{6,10},{10,14},{3,7},{... | collective-permute-start | bytes 16904 | tf_op jit(solution)/shard_map/ppermute | solution.py:18
  307.5 6.0 %collective-permute-start.1 = (bf16[1,2816]{1,0:T(2,128)(2,1)S(1)}, bf16[1,2816]{1,0:T(2,128)(2,1)S(1)}, u32[]{:S(2)}, u32[]{:S(2)}) collective-permute-start(bf16[1,2816]{1,0:T(2,128)(2,1)S(1)} %get-tuple-element.14), channel_id=1, source_target_pairs={{4,0},{8,4},{12,8},{5,1},{9,5},{13,9},{6,2},{10,6},{14,10},{7,3},{... | collective-permute-start | bytes 16904 | tf_op jit(solution)/shard_map/ppermute | solution.py:21
  398.6 49.3 %copy-start.1 = (bf16[768,256]{1,0:T(8,128)(2,1)S(1)}, bf16[768,256]{1,0:T(8,128)(2,1)}, u32[]{:S(2)}) copy-start(bf16[768,256]{1,0:T(8,128)(2,1)} %param.16) | copy-start | bytes 1179652
Sparse Core Ops, SparseCore 0:
  8.9 37.1 all-gather.5
  47.7 107.3 all-gather.9
  156.7 105.2 all-gather.11
  263.4 26.7 all-gather.7
  291.6 106.9 all-gather.13
  409.5 36.0 reduce-scatter.1
where the time goes:
time: 455 us
  waiting for transfers between devices  315 us (69%)
  blocking collectives  49.6 us (11%)
  matrix products  45.2 us (10%)
  other arithmetic  24.4 us (5%)
  between operations  13.8 us (3%)
  starting transfers between devices  4.88 us (1%)
    all_gather x1, waiting for transfers between devices, body(): lax.all_gather(value_in, 'sp', axis=0, tiled=True)  107 us
    all_gather x1, waiting for transfers between devices, body(): lax.all_gather(down_t, 'sp', axis=0, tiled=True)  79.2 us
    all_gather x1, waiting for transfers between devices, body(): lax.all_gather(gate_in, 'sp', axis=0, tiled=True)  57.5 us
    reduce_scatter x1, waiting for transfers between devices, body(): lax.psum_scatter(lax.dot_general(hidden, down_rows, (((1,), (1,)), ((), (...  36.2 us
    all_gather x1, waiting for transfers between devices, body(): lax.all_gather(normed, 'tp', axis=0, tiled=True)  28.2 us
    all_gather x1, blocking collectives, body(): key_piece = lax.all_gather(key_rot, 'sp', axis=0, tiled=True)  21.3 us
    all_gather x1, blocking collectives, body(): value_piece = lax.all_gather(value_own, 'sp', axis=0, tiled=True)  18.4 us
    dot_general x1, matrix products, body(): jnp.dot(lax.all_gather(normed, 'tp', axis=0, tiled=True), paired, preferr...  13.8 us
  transfers between devices with their start and end apart: 8, of which 7 were waited for; matrix products, arithmetic and copies ran while one was open for 13% of the time, Pallas kernels for 0%

commit v1 on v0

--- a/solution.py
+++ b/solution.py
@@ -93,8 +93,11 @@
     query_rows = jnp.transpose(query_rot, (1, 0, 2)).reshape(local_heads * tok_rows, head_dim)
     query_count = local_heads * tok_rows
     running = jnp.full((query_count, 1), -1e30, jnp.float32)
-    key_piece = lax.all_gather(key_rot, "sp", axis=0, tiled=True)
-    value_piece = lax.all_gather(value_own, "sp", axis=0, tiled=True)
+    key_piece, value_piece = jnp.split(
+        jax.lax.all_gather(jnp.concatenate([key_rot, value_own], axis=1), "sp", axis=0, tiled=True),
+        [key_rot.shape[1]],
+        axis=1,
+    )
     scores = lax.dot_general(
         query_rows, key_piece, (((1,), (1,)), ((), ())), preferred_element_type=jnp.float32
     )

time: 455 us -> 496 us (1.090)
  waiting for transfers between devices: 315 us -> 393 us
  blocking collectives: 49.6 us -> 9.89 us
    all_gather x1, waiting for transfers between devices: 57.5 us -> 99.1 us  [body(): lax.all_gather(gate_in, 'sp', axis=0, tiled=True)]
    all_gather x2 -> x0, blocking collectives: 39.7 us -> none  [the longest x1 21.3 us: body(): key_piece = lax.all_gather(key_rot, 'sp', axis=0, tiled=True)]
    all_gather x0 -> x1, waiting for transfers between devices: none -> 36.4 us  [body(): jax.lax.all_gather(jnp.concatenate([key_rot, value_own], axis=1), 'sp', a...]
  transfers between devices with their start and end apart: 8 -> 9, of which waited for: 7 -> 8; matrix products, arithmetic and copies ran while one was open for 13% -> 11% of each run, Pallas kernels for 0% -> 0%
where the time goes in v1:
time: 496 us; the launch traced here: 495 us
  waiting for transfers between devices  393 us (79%)
  matrix products  47 us (9%)
  other arithmetic  25.6 us (5%)
  between operations  13.9 us (3%)
  blocking collectives  9.89 us (2%)
    all_gather x1, waiting for transfers between devices, body(): lax.all_gather(value_in, 'sp', axis=0, tiled=True)  106 us
    all_gather x1, waiting for transfers between devices, body(): lax.all_gather(gate_in, 'sp', axis=0, tiled=True)  99.1 us
    all_gather x1, waiting for transfers between devices, body(): lax.all_gather(down_t, 'sp', axis=0, tiled=True)  79.1 us
    all_gather x1, waiting for transfers between devices, body(): jax.lax.all_gather(jnp.concatenate([key_rot, value_own], axis=1), 'sp', a...  36.4 us
    reduce_scatter x1, waiting for transfers between devices, body(): lax.psum_scatter(lax.dot_general(hidden, down_rows, (((1,), (1,)), ((), (...  36.2 us
    all_gather x1, waiting for transfers between devices, body(): lax.all_gather(normed, 'tp', axis=0, tiled=True)  28.2 us
    dot_general x1, matrix products, body(): jnp.dot(lax.all_gather(normed, 'tp', axis=0, tiled=True), paired, preferr...  13.8 us
    dot_general x1, matrix products, body(): lax.dot_general(hidden, down_rows, (((1,), (1,)), ((), ())), preferred_el...  10.7 us
  transfers between devices with their start and end apart: 9, of which 8 were waited for; matrix products, arithmetic and copies ran while one was open for 11% of the time, Pallas kernels for 0%

profile of v1, /device:TPU:0, one launch (start us, length us, event | category | flops | bytes accessed | tf_op | source)
XLA Modules:
  0.0 495.4 jit_solution(6911770089833920316)
XLA Ops:
  6.6 1.2 fusion.46
  7.8 1.1 fusion.47
  8.9 0.4 slice_negate_fusion.1
  9.3 0.3 broadcast_multiply_fusion.1
  9.6 2.0 fusion.49
  11.6 0.8 pad_maximum_fusion.1
  12.5 0.0 all-gather.9.cloned.1.call-start
  12.5 0.7 all-gather.9.cloned.1.call-update
  13.3 0.7 all-gather.13.cloned.1.call-update
  14.0 0.5 all-gather.15.cloned.1.call-update
  14.5 0.0 all-gather.11.cloned.1.call-start
  14.6 0.2 copy.18
  14.7 0.2 copy.19
  14.9 0.2 copy.17
  15.1 0.1 fusion.38
  15.2 0.1 fusion.39
  15.4 0.1 slice_negate_fusion.3
  15.4 0.3 fusion.51
  15.7 0.2 copy.20
  15.9 36.4 %all-gather.7.cloned.1.call-done = bf16[3072,256]{1,0:T(8,128)(2,1)} async-done(((bf16[768,256]{1,0:T(8,128)(2,1)}), bf16[3072,256]{1,0:T(8,128)(2,1)}) %all-gather.7.cloned.1.call-update) | async-done | bytes 1572880 | tf_op jit(solution)/shard_map/all_gather | solution.py:97
  52.4 9.9 %fusion.71 = (f32[1536]{0:T(1024)S(1)}, f32[1536,3072]{1,0:T(8,128)}) fusion(bf16[1536,128]{1,0:T(8,128)(2,1)S(1)} %bitcast.22, bf16[3072,256]{1,0:T(8,128)(2,1)} %all-gather.7.cloned.1.call-done), kind=kOutput, calls=%fused_computation.108 | convolution fusion | flops 1212676608 | bytes 20060160 | tf_op jit(solution)/shard_map/dot_general | solution.py:101
  62.2 9.1 %fusion = f32[1536]{0:T(1024)S(1)} fusion(f32[1536,3072]{1,0:T(8,128)} %get-tuple-element.26, f32[1536]{0:T(1024)S(1)} %broadcast_maximum_fusion), kind=kLoop, calls=%fused_computation.1 | loop fusion | flops 9435648 | bytes 18886656 | tf_op jit(solution)/shard_map/reduce_sum | solution.py:106
  71.4 9.3 %fusion.26 = bf16[1536,128]{1,0:T(8,128)(2,1)S(1)} fusion(f32[1536,3072]{1,0:T(8,128)} %get-tuple-element.26, f32[1536]{0:T(1024)S(1)} %broadcast_maximum_fusion, bf16[3072,256]{1,0:T(8,128)(2,1)S(1)} %copy-done.2, f32[1536]{0:T(1024)S(1)} %fusion), kind=kOutput, calls=%fused_computation.30 | convolution fusion | flops 1217789952 | bytes 20070400 | tf_op jit(solution)/shard_map/dot_general | solution.py:107
  80.7 0.4 copy.21
  81.1 0.3 all_to_all.12
  81.3 9.9 %all_to_all.16 = bf16[4,192,256]{2,1,0:T(8,128)(2,1)S(1)} all-to-all(bf16[4,192,256]{2,1,0:T(8,128)(2,1)S(1)} %all_to_all.12), channel_id=1, replica_groups=mesh['grp'=2,'sp'=4,'tp'=4] {'tp'}, dimensions={0} | all-to-all | bytes 786432 | tf_op jit(solution)/shard_map/all_to_all | solution.py:112
  91.2 3.3 convert_reduce_fusion
  94.6 0.2 multiply_reduce_fusion
  94.8 0.5 fusion.34
  95.3 1.1 fusion.36
  96.5 0.0 all-gather.17.cloned.1.call-start
  96.5 0.5 all-gather.17.cloned.1.call-update
  97.1 0.0 reduce-scatter.2.cloned.1.call-start
  97.2 99.1 %all-gather.13.cloned.1.call-done = bf16[2048,1408]{1,0:T(8,128)(2,1)} async-done(((bf16[512,1408]{1,0:T(8,128)(2,1)}), bf16[2048,1408]{1,0:T(8,128)(2,1)}) %all-gather.13.cloned.1.call-update) | async-done | bytes 5767184 | tf_op jit(solution)/shard_map/all_gather | solution.py:71
  196.2 106.4 %all-gather.15.cloned.1.call-done = bf16[2048,1408]{1,0:T(8,128)(2,1)} async-done(((bf16[512,1408]{1,0:T(8,128)(2,1)}), bf16[2048,1408]{1,0:T(8,128)(2,1)}) %all-gather.15.cloned.1.call-update) | async-done | bytes 5767184 | tf_op jit(solution)/shard_map/all_gather | solution.py:72
  302.6 28.2 %all-gather.11.cloned.1.call-done = bf16[768,2048]{1,0:T(8,128)(2,1)} async-done(((bf16[192,2048]{1,0:T(8,128)(2,1)}), bf16[768,2048]{1,0:T(8,128)(2,1)}) %all-gather.11.cloned.1.call-update) | async-done | bytes 3145744 | tf_op jit(solution)/shard_map/all_gather | solution.py:125
  330.8 13.8 %fusion.11 = bf16[768,2816]{1,0:T(8,128)(2,1)S(1)} fusion(bf16[768,2048]{1,0:T(8,128)(2,1)} %all-gather.11.cloned.1.call-done, bf16[2048,1408]{1,0:T(8,128)(2,1)} %all-gather.15.cloned.1.call-done, bf16[2048,1408]{1,0:T(8,128)(2,1)} %all-gather.13.cloned.1.call-done), kind=kOutput, calls=%fused_computation.16 | convolution fusion | flops 8883601408 | bytes 19005440 | tf_op jit(solution)/shard_map/dot_general | solution.py:124
  344.7 3.4 collective-permute-start
  348.1 1.3 collective-permute-start.1
  349.4 0.1 slice_reduce_fusion.2
  349.5 0.2 collective-permute-done
  349.7 4.5 collective-permute-done.1
  354.1 1.2 maximum_convert_fusion
  355.3 4.8 fusion.9
  360.1 79.1 %all-gather.17.cloned.1.call-done = bf16[2048,1408]{1,0:T(8,128)(2,1)} async-done(((bf16[512,1408]{1,0:T(8,128)(2,1)}), bf16[2048,1408]{1,0:T(8,128)(2,1)}) %all-gather.17.cloned.1.call-update) | async-done | bytes 5767184 | tf_op jit(solution)/shard_map/all_gather | solution.py:73
  439.2 10.7 %convolution_convert_fusion.1 = bf16[768,2048]{1,0:T(8,128)(2,1)} fusion(bf16[2048,1408]{1,0:T(8,128)(2,1)} %all-gather.17.cloned.1.call-done, f32[768,2816]{1,0:T(8,128)} %fusion.9), kind=kOutput, calls=%fused_computation.28 | convolution fusion | flops 4441571328 | bytes 17563648 | tf_op jit(solution)/shard_map/dot_general | solution.py:135
  450.0 36.2 %reduce-scatter.2.cloned.1.call-done = bf16[192,2048]{1,0:T(8,128)(2,1)} async-done(((bf16[768,2048]{1,0:T(8,128)(2,1)}), bf16[192,2048]{1,0:T(8,128)(2,1)}) %reduce-scatter.2.cloned.1.call-update) | async-done | bytes 786448 | tf_op jit(solution)/shard_map/reduce_scatter | solution.py:134
  486.2 2.3 fusion.37
  (42 shorter events, 0.3 us)
Async XLA Ops:
  6.5 2.8 copy-start
  6.5 3.1 copy-start.3
  6.5 3.1 copy-start.10
  6.5 45.8 %all-gather.7.cloned.1.call-start = ((), (), s32[]{:S(2)}) async-start(), calls=%async_computation.2 | async-start | bytes 1966080 | tf_op jit(solution)/shard_map/all_gather | solution.py:97
  9.6 5.3 %copy-start.5 = (bf16[768,256]{1,0:T(8,128)(2,1)S(1)}, bf16[768,256]{1,0:T(8,128)(2,1)}, u32[]{:S(2)}) copy-start(bf16[768,256]{1,0:T(8,128)(2,1)} %param.14) | copy-start | bytes 1179652
  11.6 3.6 copy-start.11
  12.5 78.8 %all-gather.9.cloned.1.call-start = ((), (), s32[]{:S(2)}) async-start(), calls=%async_computation.3 | async-start | bytes 5242880 | tf_op jit(solution)/shard_map/all_gather | solution.py:75
  13.2 183.0 %all-gather.13.cloned.1.call-start = ((), (), s32[]{:S(2)}) async-start(), calls=%async_computation.5 | async-start | bytes 7208960 | tf_op jit(solution)/shard_map/all_gather | solution.py:71
  14.0 288.7 %all-gather.15.cloned.1.call-start = ((), (), s32[]{:S(2)}) async-start(), calls=%async_computation.6 | async-start | bytes 7208960 | tf_op jit(solution)/shard_map/all_gather | solution.py:72
  14.5 316.3 %all-gather.11.cloned.1.call-start = ((), (), s32[]{:S(2)}) async-start(), calls=%async_computation.4 | async-start | bytes 3932160 | tf_op jit(solution)/shard_map/all_gather | solution.py:125
  62.2 9.2 %copy-start.2 = (bf16[3072,256]{1,0:T(8,128)(2,1)S(1)}, bf16[3072,256]{1,0:T(8,128)(2,1)}, u32[]{:S(2)}) copy-start(bf16[3072,256]{1,0:T(8,128)(2,1)} %all-gather.7.cloned.1.call-done) | copy-start | bytes 4718596
  91.2 3.6 copy-start.4
  91.2 3.6 copy-start.8
  94.6 0.7 copy-start.9
  94.6 2.5 copy-start.6
  94.6 2.5 copy-start.7
  96.5 342.7 %all-gather.17.cloned.1.call-start = ((), (), s32[]{:S(2)}) async-start(), calls=%async_computation.7 | async-start | bytes 7208960 | tf_op jit(solution)/shard_map/all_gather | solution.py:73
  97.1 389.2 %reduce-scatter.2.cloned.1.call-start = ((), (), s32[]{:S(2)}) async-start(), calls=%async_computation.8 | async-start | bytes 3932160 | tf_op jit(solution)/shard_map/reduce_scatter | solution.py:134
  344.7 4.9 collective-permute-start
  348.1 6.0 %collective-permute-start.1 = (bf16[1,2816]{1,0:T(2,128)(2,1)S(1)}, bf16[1,2816]{1,0:T(2,128)(2,1)S(1)}, u32[]{:S(2)}, u32[]{:S(2)}) collective-permute-start(bf16[1,2816]{1,0:T(2,128)(2,1)S(1)} %get-tuple-element.14), channel_id=1, source_target_pairs={{4,0},{8,4},{12,8},{5,1},{9,5},{13,9},{6,2},{10,6},{14,10},{7,3},{... | collective-permute-start | bytes 16904 | tf_op jit(solution)/shard_map/ppermute | solution.py:21
  439.2 49.3 %copy-start.1 = (bf16[768,256]{1,0:T(8,128)(2,1)S(1)}, bf16[768,256]{1,0:T(8,128)(2,1)}, u32[]{:S(2)}) copy-start(bf16[768,256]{1,0:T(8,128)(2,1)} %param.16) | copy-start | bytes 1179652
Sparse Core Ops, SparseCore 0:
  12.6 39.7 all-gather.6
  53.9 33.3 all-gather.8
  88.9 107.3 all-gather.12
  197.7 104.9 all-gather.14
  304.0 26.7 all-gather.10
  332.3 106.9 all-gather.16
  450.1 36.0 reduce-scatter.1
